TPU v7x, 512 devices: a 8x2x16 block of a 8x8x16 slice. The times are simulated.
512 devices in a mesh: grp: 2 (over y), sp: 32 (over z, core), tp: 8 (over x).
Axes of the slice: x: 8, y: 2, z: 16, core: 2. Of those that a mesh axis runs over, the one named last changes fastest.
The devices are a block of a 8x8x16 slice.
Arguments:
- out_gate: bfloat16 [24576, 1024], P(('grp', 'sp'), 'tp'), parts along dimension 0, may hold values from -6 to 6
- in_gate: bfloat16 [24576, 1024], P(('grp', 'sp'), 'tp'), parts along dimension 0, may hold values from -6 to 6
- conv_input: bfloat16 [24576, 1024], P(('grp', 'sp'), 'tp'), parts along dimension 0, may hold values from -6 to 6
- doc_ids: int32 [24576], P(('grp', 'sp')), parts along dimension 0, may hold values from 0 to 15, never falling along the last dimension, each value on 1 to 1536 neighbouring positions
- residual: bfloat16 [24576, 2048], P(('grp', 'sp'), 'tp'), parts along dimension 0, may hold values from -6 to 6
- conv_taps: float32 [3, 1024], P(None, 'tp'), may hold values from -6 to 6
- mix_gain: float32 [1024], P('tp'), may hold values from 0.1 to 1.9
- out_weight: bfloat16 [1024, 2048], P('tp'), may hold values from -0.1875 to 0.1875
- ffn_gain: float32 [2048], P('tp'), may hold values from 0.1 to 1.9
- routing: int32 [24576, 2], P(('grp', 'sp')), parts along dimension 0, may hold values from 0 to 63, as said below
- route_weight: float32 [24576, 2], P(('grp', 'sp')), parts along dimension 0, may hold values from 0.2 to 1.2
- expert_gate: bfloat16 [64, 2048, 512], P('sp', None, 'tp'), may hold values from -0.125 to 0.125
- expert_up: bfloat16 [64, 2048, 512], P('sp', None, 'tp'), may hold values from -0.125 to 0.125
- expert_down: bfloat16 [64, 512, 2048], P('sp', None, 'tp'), may hold values from -0.25 to 0.25
- shared_gate: bfloat16 [2048, 512], P(None, 'tp'), may hold values from -0.125 to 0.125
- shared_up: bfloat16 [2048, 512], P(None, 'tp'), may hold values from -0.125 to 0.125
- shared_down: bfloat16 [512, 2048], P(None, 'tp'), may hold values from -0.25 to 0.25
Outputs:
- layer_out: bfloat16 [24576, 2048], P(('grp', 'sp'), 'tp'), parts along dimension 0
There are 2 independent parts, one for each index of `grp`. A program takes and returns all parts, laid end to end along the dimension named above; an argument that names none is the same for every part. Nothing has to cross between parts.
Inputs may be any that keep to these rules, and one draw needn't show every extreme that they name: `routing`: each row names 2 different experts. In each aligned block of 48 rows no expert is named by more than 3 rows, and some expert is named by exactly 3 rows. `doc_ids`: never falls along the sequence; a document holds at most 1536 positions.
All inputs are finite; a program needn't handle non-finite values.
Results may differ from a plain program's by a relative error of at most 0.017.
Values may be sent and summed in bfloat16 or wider, within the bound.
No kernel may reach another device: no remote copies, remote signals or barrier semaphores. Data moves between devices by JAX's collectives and lax.ppermute only.
A program may use at most 64 MiB of HBM per device.

v0:
```python
import jax
import jax.numpy as jnp
from jax import lax
from jax.sharding import PartitionSpec as P

D_CONV = 1024
CONV_K = 3
TOPK = 2
EXP_DEV = 2


def from_behind(value, axis, steps):
    count = lax.axis_size(axis)
    first, last = (max(0, -steps), min(count, count - steps))
    return lax.ppermute(value, axis, [(source, source + steps) for source in range(first, last)])


def sent_to_all(shard, axis):
    copies = jnp.broadcast_to(shard, (lax.axis_size(axis), *shard.shape))
    return lax.all_to_all(copies, axis, split_axis=0, concat_axis=0, tiled=True)


def of_everyone(shard, axis):
    return sent_to_all(shard, axis).sum(axis=0)


def cut_along(shard, dim, length):
    shape = shard.shape
    pieces = shard.reshape(*shape[:dim], length, shape[dim] // length, *shape[dim + 1 :])
    return jnp.moveaxis(pieces, dim, 0)


def sum_at_owner(shard, axis, dim):
    pieces = cut_along(shard, dim, lax.axis_size(axis))
    arrived = lax.all_to_all(pieces, axis, split_axis=0, concat_axis=0, tiled=True)
    return arrived.astype(jnp.float32).sum(axis=0)


def rows_first(arrays, axis, dims):
    turned = [jnp.moveaxis(a, dim, 0) for a, dim in zip(arrays, dims)]
    both = jnp.concatenate([t.reshape(len(t), -1) for t in turned], axis=1)
    whole, at, finished = (lax.all_gather(both, axis, axis=0, tiled=True), 0, [])
    for t, dim in zip(turned, dims):
        slab = whole[:, at : at + t[0].size].reshape(-1, *t.shape[1:])
        finished.append(jnp.moveaxis(slab, 0, dim))
        at += t[0].size
    return tuple(finished)


def body(
    out_gate,
    in_gate,
    conv_input,
    doc_ids,
    residual,
    conv_taps,
    mix_gain,
    out_weight,
    ffn_gain,
    routing,
    route_weight,
    expert_gate,
    expert_up,
    expert_down,
    shared_gate,
    shared_up,
    shared_down,
):
    tokens = residual.shape[0]
    width = out_weight.shape[1]
    n_tp = lax.axis_size("tp")
    n_sp = lax.axis_size("sp")
    rows = tokens // n_tp
    experts = n_sp * EXP_DEV
    most = max(1, 2 * rows * TOPK // experts)
    slots = n_tp * most
    total = experts * slots
    cols = expert_down.shape[2]
    product = (in_gate.astype(jnp.float32) * conv_input.astype(jnp.float32)).astype(jnp.bfloat16)
    tail = (product[tokens - CONV_K + 1 :], doc_ids[tokens - CONV_K + 1 :].astype(jnp.bfloat16))
    prev_rows, prev_docs = from_behind((tail[0], tail[1]), "sp", 1)
    extended = jnp.concatenate([prev_rows, product], axis=0).astype(jnp.float32)
    ext_docs = jnp.concatenate([prev_docs.astype(jnp.int32), doc_ids])
    mixed = jnp.zeros(product.shape, jnp.float32)
    for k in range(CONV_K):
        keep = (ext_docs[k : k + tokens] == doc_ids)[:, None]
        mixed = mixed + jnp.where(keep, conv_taps[k] * extended[k : k + tokens], jnp.float32(0.0))
    conv_out = out_gate.astype(jnp.float32) * mixed
    squares = of_everyone(jnp.sum(conv_out * conv_out, axis=1), "tp")
    normed = (conv_out * lax.rsqrt(squares / D_CONV + 1e-06)[:, None] * mix_gain).astype(
        jnp.bfloat16
    )
    partial_value = jnp.dot(normed, out_weight, preferred_element_type=jnp.float32)
    proj = sum_at_owner(partial_value.astype(jnp.bfloat16), "tp", 1)
    stream = (residual.astype(jnp.float32) + proj).astype(jnp.bfloat16)
    stream32 = stream.astype(jnp.float32)
    stream_sq = of_everyone(jnp.sum(stream32 * stream32, axis=1), "tp")
    normal_cols = (stream32 * lax.rsqrt(stream_sq / width + 1e-06)[:, None] * ffn_gain).astype(
        jnp.bfloat16
    )
    flat_expert = routing.reshape(-1)
    onehot = (flat_expert[:, None] == jnp.arange(experts, dtype=jnp.int32)[None, :]).astype(
        jnp.int32
    )
    blocked = onehot.reshape(n_tp, rows * TOPK, experts)
    earlier = jnp.cumsum(blocked, axis=1) - blocked
    position = jnp.sum(earlier * blocked, axis=2).reshape(-1)
    entry = jnp.arange(tokens * TOPK, dtype=jnp.int32)
    slot = flat_expert * slots + entry // (rows * TOPK) * most + position
    table = jnp.full((total,), tokens, jnp.int32).at[slot].set(entry // TOPK)
    block_rows = lax.all_to_all(normal_cols, "tp", split_axis=0, concat_axis=1, tiled=True)
    mine = lax.dynamic_index_in_dim(
        table.reshape(n_sp, EXP_DEV, n_tp, most), lax.axis_index("tp"), 2, False
    )
    local = jnp.where(mine >= tokens, rows, mine - lax.axis_index("tp") * rows)
    padded_block = jnp.concatenate([block_rows, jnp.zeros((1, width), jnp.bfloat16)], axis=0)
    got = lax.all_to_all(padded_block[local], "sp", split_axis=0, concat_axis=0, tiled=True)
    arrived, whole = (
        lax.all_gather(got, "tp", axis=2, tiled=True),
        lax.all_gather(block_rows.reshape(1, 1, rows, width), "tp", axis=2, tiled=True),
    )
    normal = whole.reshape(tokens, width)
    gate = jnp.einsum("nesd,edh->nesh", arrived, expert_gate, preferred_element_type=jnp.float32)
    upper = jnp.einsum("nesd,edh->nesh", arrived, expert_up, preferred_element_type=jnp.float32)
    hidden = (jax.nn.silu(gate) * upper).astype(jnp.bfloat16)
    hidden_flat = hidden.reshape(n_sp * EXP_DEV * slots, hidden.shape[3])
    shared_hid = (
        jax.nn.silu(jnp.dot(normal, shared_gate, preferred_element_type=jnp.float32))
        * jnp.dot(normal, shared_up, preferred_element_type=jnp.float32)
    ).astype(jnp.bfloat16)
    expert_piece, shared_piece = rows_first((hidden_flat, shared_hid), "tp", (1, 1))
    count = expert_piece.shape[1]
    expert_part = jnp.einsum(
        "nesh,ehd->nesd",
        expert_piece.reshape(n_sp, EXP_DEV, slots, count),
        expert_down,
        preferred_element_type=jnp.float32,
    )
    shared_part = jnp.dot(shared_piece, shared_down, preferred_element_type=jnp.float32)
    returned = lax.all_to_all(
        expert_part.astype(jnp.bfloat16), "sp", split_axis=0, concat_axis=0, tiled=True
    )
    picked = (
        returned.reshape(total, cols)[slot].astype(jnp.float32) * route_weight.reshape(-1)[:, None]
    )
    routed = jnp.sum(picked.reshape(tokens, TOPK, cols), axis=1)
    return (stream32 + shared_part + routed).astype(jnp.bfloat16)


def solution(mesh):
    return jax.shard_map(
        body,
        mesh=mesh,
        in_specs=(
            P(("grp", "sp"), "tp"),
            P(("grp", "sp"), "tp"),
            P(("grp", "sp"), "tp"),
            P(("grp", "sp")),
            P(("grp", "sp"), "tp"),
            P(None, "tp"),
            P("tp"),
            P("tp", None),
            P("tp"),
            P(("grp", "sp"), None),
            P(("grp", "sp"), None),
            P("sp", None, "tp"),
            P("sp", None, "tp"),
            P("sp", None, "tp"),
            P(None, "tp"),
            P(None, "tp"),
            P(None, "tp"),
        ),
        out_specs=P(("grp", "sp"), "tp"),
        check_vma=False,
    )
```

profile of v0, /device:TPU:65, one launch (start us, length us, event | category | flops | bytes accessed | tf_op | source)
XLA Modules:
  0.0 412.4 jit_solution(5063214200456433942)
XLA Ops:
  6.6 1.0 multiply_convert_fusion.1
  7.6 7.1 %collective-permute-start.1 = (bf16[2,128]{1,0:T(2,128)(2,1)S(1)}, bf16[2,128]{1,0:T(2,128)(2,1)S(1)}, u32[]{:S(2)}, u32[]{:S(2)}) collective-permute-start(bf16[2,128]{1,0:T(2,128)(2,1)S(1)} %slice.53), channel_id=1, source_target_pairs={{0,8},{8,16},{16,24},{24,32},{32,40},{40,48},{48,56},{56,64},{64,7... | collective-permute-start | bytes 1544 | tf_op jit(solution)/shard_map/ppermute | solution.py:15
  14.7 0.7 convert.4
  15.4 1.9 collective-permute-start
  17.4 0.8 slice_bitcast_fusion.2
  18.2 34.9 %collective-permute-done = bf16[2]{0:T(256)(128)(2,1)S(1)} collective-permute-done((bf16[2]{0:T(256)(128)(2,1)S(1)}, bf16[2]{0:T(256)(128)(2,1)S(1)}, u32[]{:S(2)}, u32[]{:S(2)}) %collective-permute-start) | collective-permute-done | bytes 36 | tf_op jit(solution)/shard_map/ppermute | solution.py:15
  53.0 0.8 pad_add_fusion
  53.8 0.8 slice_compare_fusion.1
  54.6 1.2 multiply_reduce_fusion.1
  55.8 9.1 %all_to_all.46 = f32[8,1,384]{2,1,0:T(1,128)S(1)} all-to-all(f32[8,1,384]{2,1,0:T(1,128)S(1)} %broadcast_in_dim.50), channel_id=1, replica_groups=mesh['grp'=2,'sp'=32,'tp'=8] {'tp'}, dimensions={0} | all-to-all | bytes 24576 | tf_op jit(solution)/shard_map/all_to_all | solution.py:20
  64.9 0.6 convolution_convert_fusion
  65.5 1.3 copy.114
  66.8 3.9 all-to-all-start.1
  71.1 1.9 select_reduce_fusion
  73.5 35.1 %all-to-all-done.1 = bf16[8,384,256]{2,1,0:T(8,128)(2,1)S(1)} async-done(((bf16[8,384,256]{2,1,0:T(8,128)(2,1)}), bf16[8,384,256]{2,1,0:T(8,128)(2,1)S(1)}, u32[]{:S(2)}, u32[]{:S(2)}) %all-to-all-start.1) | async-done | bytes 1572896 | tf_op jit(solution)/shard_map/all_to_all | solution.py:35
  109.0 0.6 broadcast_in_dim.51
  109.6 3.7 all-to-all-start.2
  113.3 3.4 scatter_custom_fusion
  116.9 3.0 all-to-all-done.2
  120.0 0.8 fusion.51
  120.8 3.7 all-to-all-start.3
  124.7 8.5 %all-to-all-done.3 = bf16[8,48,256]{2,1,0:T(8,128)(2,1)S(1)} async-done(((bf16[8,48,256]{2,1,0:T(8,128)(2,1)}), bf16[8,48,256]{2,1,0:T(8,128)(2,1)S(1)}, u32[]{:S(2)}, u32[]{:S(2)}) %all-to-all-start.3) | async-done | bytes 196640 | tf_op jit(solution)/shard_map/all_to_all | solution.py:111
  133.2 1.1 gather_fusion
  134.3 0.5 reshape.189
  134.8 1.9 copy.75
  136.7 15.3 %all-to-all-start.4 = ((bf16[32,2,3,2048]{3,1,2,0:T(2,128)(2,1)}), bf16[32,2,3,2048]{3,1,2,0:T(2,128)(2,1)S(1)}, u32[]{:S(2)}, u32[]{:S(2)}) async-start(bf16[32,2,3,2048]{3,1,2,0:T(2,128)(2,1)} %copy.75), calls=%async_computation.4 | async-start | bytes 1572864 | tf_op jit(solution)/shard_map/all_to_all | solution.py:117
  152.2 0.8 reshape.183
  153.1 43.3 %all-to-all-done.4 = bf16[32,2,3,2048]{3,1,2,0:T(2,128)(2,1)S(1)} async-done(((bf16[32,2,3,2048]{3,1,2,0:T(2,128)(2,1)}), bf16[32,2,3,2048]{3,1,2,0:T(2,128)(2,1)S(1)}, u32[]{:S(2)}, u32[]{:S(2)}) %all-to-all-start.4) | async-done | bytes 786464 | tf_op jit(solution)/shard_map/all_to_all | solution.py:117
  196.4 1.2 copy.76
  197.7 0.2 all-gather.8.cloned.1.call-start
  198.0 2.1 fusion.30
  200.2 1.6 fusion.39
  201.9 76.6 %all-gather.4.cloned.1.call-done = bf16[32,2,24,2048]{3,0,1,2:T(8,128)(2,1)} async-done(((bf16[32,2,3,2048]{3,0,1,2:T(8,128)(2,1)}), bf16[32,2,24,2048]{3,0,1,2:T(8,128)(2,1)}) %all-gather.4.cloned.1.call-update) | async-done | bytes 6291472 | tf_op jit(solution)/shard_map/all_gather | solution.py:119
  278.6 4.7 %fusion.16 = f32[32,2,24,64]{3,0,2,1:T(8,128)S(1)} fusion(bf16[32,2,24,2048]{3,0,1,2:T(8,128)(2,1)} %all-gather.4.cloned.1.call-done, bf16[2,2048,64]{1,2,0:T(8,128)(2,1)S(1)} %copy-done.10), kind=kOutput, calls=%fused_computation.18 | convolution fusion | flops 402653184 | bytes 7208960 | tf_op jit(solution)/shard_map/nesd,edh->nesh/dot_general | solution.py:123
  283.3 1.8 fusion.25
  285.4 0.9 copy.82
  286.3 42.3 %all-gather.8.cloned.1.call-done = bf16[512,1920]{1,0:T(8,128)(2,1)} async-done(((bf16[64,1920]{1,0:T(8,128)(2,1)}), bf16[512,1920]{1,0:T(8,128)(2,1)}) %all-gather.8.cloned.1.call-update) | async-done | bytes 1966096 | tf_op jit(solution)/shard_map/all_gather | solution.py:42
  328.7 1.4 slice-done
  330.1 1.6 copy.92
  331.6 2.1 fusion.13
  333.7 1.0 copy.85
  334.7 18.1 %all-to-all-start.5 = ((bf16[32,2,24,256]{3,2,1,0:T(8,128)(2,1)}), bf16[32,2,24,256]{3,2,1,0:T(8,128)(2,1)S(1)}, u32[]{:S(2)}, u32[]{:S(2)}) async-start(bf16[32,2,24,256]{3,2,1,0:T(8,128)(2,1)} %copy.85), calls=%async_computation.5 | async-start | bytes 1572864 | tf_op jit(solution)/shard_map/all_to_all | solution.py:140
  352.8 0.8 copy.86
  353.6 43.6 %all-to-all-done.5 = bf16[32,2,24,256]{3,2,1,0:T(8,128)(2,1)S(1)} async-done(((bf16[32,2,24,256]{3,2,1,0:T(8,128)(2,1)}), bf16[32,2,24,256]{3,2,1,0:T(8,128)(2,1)S(1)}, u32[]{:S(2)}, u32[]{:S(2)}) %all-to-all-start.5) | async-done | bytes 786464 | tf_op jit(solution)/shard_map/all_to_all | solution.py:140
  397.2 3.3 gather_fusion.1
  400.4 1.5 reshape.187
  402.0 2.0 multiply_reduce_fusion
  403.9 1.9 fusion.29
  (65 shorter events, 2.7 us)
Async XLA Ops:
  6.5 58.3 %copy-start = (bf16[128,2048]{1,0:T(8,128)(2,1)S(1)}, bf16[128,2048]{1,0:T(8,128)(2,1)}, u32[]{:S(2)}) copy-start(bf16[128,2048]{1,0:T(8,128)(2,1)} %param.24) | copy-start | bytes 1572868
  6.6 58.3 %copy-start.8 = (f32[128]{0:T(128)S(1)}, f32[128]{0:T(128)}, u32[]{:S(2)}) copy-start(f32[128]{0:T(128)} %param.23) | copy-start | bytes 1540
  7.6 47.0 %collective-permute-start.1 = (bf16[2,128]{1,0:T(2,128)(2,1)S(1)}, bf16[2,128]{1,0:T(2,128)(2,1)S(1)}, u32[]{:S(2)}, u32[]{:S(2)}) collective-permute-start(bf16[2,128]{1,0:T(2,128)(2,1)S(1)} %slice.53), channel_id=1, source_target_pairs={{0,8},{8,16},{16,24},{24,32},{32,40},{40,48},{48,56},{56,64},{64,7... | collective-permute-start | bytes 1544 | tf_op jit(solution)/shard_map/ppermute | solution.py:15
  15.4 37.6 %collective-permute-start = (bf16[2]{0:T(256)(128)(2,1)S(1)}, bf16[2]{0:T(256)(128)(2,1)S(1)}, u32[]{:S(2)}, u32[]{:S(2)}) collective-permute-start(bf16[2]{0:T(256)(128)(2,1)S(1)} %slice.37), channel_id=1, source_target_pairs={{0,8},{8,16},{16,24},{24,32},{32,40},{40,48},{48,56},{56,64},{64,7... | collective-permute-start | bytes 20 | tf_op jit(solution)/shard_map/ppermute | solution.py:15
  66.8 3.9 copy-start.5
  66.8 41.9 %all-to-all-start.1 = ((bf16[8,384,256]{2,1,0:T(8,128)(2,1)}), bf16[8,384,256]{2,1,0:T(8,128)(2,1)S(1)}, u32[]{:S(2)}, u32[]{:S(2)}) async-start(bf16[8,384,256]{2,1,0:T(8,128)(2,1)} %bitcast.76), calls=%async_computation.1 | async-start | bytes 3145728 | tf_op jit(solution)/shard_map/all_to_all | solution.py:35
  70.7 38.2 %copy-start.4 = (bf16[384,256]{1,0:T(8,128)(2,1)S(1)}, bf16[384,256]{1,0:T(8,128)(2,1)}, u32[]{:S(2)}) copy-start(bf16[384,256]{1,0:T(8,128)(2,1)} %param.21) | copy-start | bytes 589828
  73.5 46.5 %copy-start.7 = (f32[256]{0:T(256)S(1)}, f32[256]{0:T(256)}, u32[]{:S(2)}) copy-start(f32[256]{0:T(256)} %param.25) | copy-start | bytes 3076
  109.6 10.3 %all-to-all-start.2 = ((f32[8,1,384]{2,1,0:T(1,128)}), f32[8,1,384]{2,1,0:T(1,128)S(1)}, u32[]{:S(2)}, u32[]{:S(2)}) async-start(f32[8,1,384]{2,1,0:T(1,128)} %broadcast_in_dim.51), calls=%async_computation.2 | async-start | bytes 24576 | tf_op jit(solution)/shard_map/all_to_all | solution.py:20
  120.8 12.4 %all-to-all-start.3 = ((bf16[8,48,256]{2,1,0:T(8,128)(2,1)}), bf16[8,48,256]{2,1,0:T(8,128)(2,1)S(1)}, u32[]{:S(2)}, u32[]{:S(2)}) async-start(bf16[8,48,256]{2,1,0:T(8,128)(2,1)} %bitcast.4), calls=%async_computation.3 | async-start | bytes 393216 | tf_op jit(solution)/shard_map/all_to_all | solution.py:111
  136.7 59.7 %all-to-all-start.4 = ((bf16[32,2,3,2048]{3,1,2,0:T(2,128)(2,1)}), bf16[32,2,3,2048]{3,1,2,0:T(2,128)(2,1)S(1)}, u32[]{:S(2)}, u32[]{:S(2)}) async-start(bf16[32,2,3,2048]{3,1,2,0:T(2,128)(2,1)} %copy.75), calls=%async_computation.4 | async-start | bytes 1572864 | tf_op jit(solution)/shard_map/all_to_all | solution.py:117
  152.0 46.0 %all-gather.6.cloned.1.call-start = ((), (), s32[]{:S(2)}) async-start(), calls=%async_computation.7 | async-start | bytes 1769472 | tf_op jit(solution)/shard_map/all_gather | solution.py:120
  152.2 45.8 %copy-start.3 = (bf16[2048,64]{0,1:T(8,128)(2,1)S(1)}, bf16[2048,64]{0,1:T(8,128)(2,1)}, u32[]{:S(2)}) copy-start(bf16[2048,64]{0,1:T(8,128)(2,1)} %param.31) | copy-start | bytes 786436
  153.0 125.6 %all-gather.4.cloned.1.call-start = ((), (), s32[]{:S(2)}) async-start(), calls=%async_computation.6 | async-start | bytes 7077888 | tf_op jit(solution)/shard_map/all_gather | solution.py:119
  197.7 130.9 %all-gather.8.cloned.1.call-start = ((), (), s32[]{:S(2)}) async-start(), calls=%async_computation.8 | async-start | bytes 2211840 | tf_op jit(solution)/shard_map/all_gather | solution.py:42
  198.0 2.1 copy-start.2
  200.2 78.4 %copy-start.10 = (bf16[2,2048,64]{1,2,0:T(8,128)(2,1)S(1)}, bf16[2,2048,64]{1,2,0:T(8,128)(2,1)}, u32[]{:S(2)}) copy-start(bf16[2,2048,64]{1,2,0:T(8,128)(2,1)} %param.28) | copy-start | bytes 1572868
  201.9 81.4 %copy-start.11 = (bf16[2,2048,64]{1,2,0:T(8,128)(2,1)S(1)}, bf16[2,2048,64]{1,2,0:T(8,128)(2,1)}, u32[]{:S(2)}) copy-start(bf16[2,2048,64]{1,2,0:T(8,128)(2,1)} %param.29) | copy-start | bytes 1572868
  278.6 4.7 %copy-start.9 = (bf16[32,2,24,2048]{3,0,1,2:T(8,128)(2,1)S(1)}, bf16[32,2,24,2048]{3,0,1,2:T(8,128)(2,1)}, u32[]{:S(2)}) copy-start(bf16[32,2,24,2048]{3,0,1,2:T(8,128)(2,1)} %all-gather.4.cloned.1.call-done) | copy-start | bytes 18874372
  328.6 1.4 slice-start
  333.7 19.0 %copy-start.6 = (f32[384,2]{0,1:T(2,128)S(1)}, f32[384,2]{0,1:T(2,128)}, u32[]{:S(2)}) copy-start(f32[384,2]{0,1:T(2,128)} %param.27) | copy-start | bytes 9220
  334.7 62.5 %all-to-all-start.5 = ((bf16[32,2,24,256]{3,2,1,0:T(8,128)(2,1)}), bf16[32,2,24,256]{3,2,1,0:T(8,128)(2,1)S(1)}, u32[]{:S(2)}, u32[]{:S(2)}) async-start(bf16[32,2,24,256]{3,2,1,0:T(8,128)(2,1)} %copy.85), calls=%async_computation.5 | async-start | bytes 1572864 | tf_op jit(solution)/shard_map/all_to_all | solution.py:140
  400.4 3.5 copy-start.1
Sparse Core Ops, SparseCore 0:
  154.9 37.8 all-gather.5
  197.8 80.6 all-gather.3
  286.5 42.1 all-gather.7
where the time goes:
time: 413 us; the launch traced here: 412 us
  waiting for transfers between devices  287 us (69%)
  starting transfers between devices  54 us (13%)
  local copies, waits for them, and re-layouts  23.7 us (6%)
  matrix products  14.9 us (4%)
  between operations  13.6 us (3%)
  other arithmetic  9.74 us (2%)
  blocking collectives  9.06 us (2%)
    all_gather x1, waiting for transfers between devices, body(): lax.all_gather(got, 'tp', axis=2, tiled=True)  76.6 us
    all_to_all x1, waiting for transfers between devices, body(): lax.all_to_all(expert_part.astype(jnp.bfloat16), 'sp', split_axis=0, conc...  43.6 us
    all_to_all x1, waiting for transfers between devices, body(): lax.all_to_all(padded_block[local], 'sp', split_axis=0, concat_axis=0, ti...  43.3 us
    all_gather x1, waiting for transfers between devices, rows_first(): lax.all_gather(both, axis, axis=0, tiled=True)  42.3 us
    all_to_all x1, waiting for transfers between devices, sum_at_owner(): lax.all_to_all(pieces, axis, split_axis=0, concat_axis=0, tiled=True)  35.1 us
    ppermute x2, waiting for transfers between devices, from_behind(): lax.ppermute(value, axis, [(source, source + steps) for source in range(f...  34.9 us
    all_to_all x1, starting transfers between devices, body(): lax.all_to_all(expert_part.astype(jnp.bfloat16), 'sp', split_axis=0, conc...  18.1 us
    all_to_all x1, starting transfers between devices, body(): lax.all_to_all(padded_block[local], 'sp', split_axis=0, concat_axis=0, ti...  15.3 us
  transfers between devices with their start and end apart: 10, of which 8 were waited for; matrix products, arithmetic and copies ran while one was open for 4% of the time, Pallas kernels for 0%

commit v1 on v0

v1 whole, which is shorter than its diff:
```python
import jax
import jax.numpy as jnp
from jax import lax
from jax.experimental import pallas as pl
from jax.experimental.pallas import tpu as pltpu
from jax.sharding import PartitionSpec as P

CONV_K = 3
TOPK = 2
EXP_DEV = 2
LANES = 128
EPS = 1e-06


def split_bf16(value, count):
    pieces, rest = [], value
    for _ in range(count):
        piece = lax.reduce_precision(rest, 8, 7)
        pieces.append(piece)
        rest = rest - piece
    return pieces


def ring_all(shard, axis):
    n = lax.axis_size(axis)
    ahead = [(i, (i - 1) % n) for i in range(n)]
    behind = [(i, (i + 1) % n) for i in range(n)]
    got = {0: shard}
    up = down = shard
    for step in range(1, (n - 1) // 2 + 1):
        up = lax.ppermute(up, axis, ahead)
        down = lax.ppermute(down, axis, behind)
        got[step], got[n - step] = up, down
    if n % 2 == 0:
        half = shard.shape[0] // 2
        if n > 2:
            first = lax.ppermute(up[:half], axis, ahead)
            second = lax.ppermute(down[half:], axis, behind)
        else:
            first = lax.ppermute(shard[:half], axis, ahead)
            second = lax.ppermute(shard[half:], axis, behind)
        got[n // 2] = jnp.concatenate([first, second], axis=0)
    return [got[d] for d in range(n)]


def hidden_kernel(group, most, x_ref, gain_ref, w_ref, out_ref, normal_ref):
    rows = x_ref.shape[0]

    @pl.when(pl.program_id(0) == 0)
    def _():
        x = x_ref[...].astype(jnp.float32)
        mean = jnp.sum(x * x, axis=1, keepdims=True) / x.shape[1]
        normal_ref[...] = (x * lax.rsqrt(mean + EPS) * gain_ref[...]).astype(jnp.bfloat16)

    normal = normal_ref[...]
    half = w_ref.shape[1] // 2

    def shard(i):
        both = lax.dot_general(
            normal, w_ref[i], (((1,), (1,)), ((), ())), preferred_element_type=jnp.float32
        )
        gate, upper = both[:, :half], both[:, half:]
        return gate / (1.0 + jnp.exp(-gate)) * upper

    a, b = shard(0), shard(1)
    second = lax.broadcasted_iota(jnp.int32, (rows, half), 0) % group >= most
    low = lax.broadcasted_iota(jnp.int32, (rows, half), 1) < half // 2
    turned = pltpu.roll(jnp.where(second, a, b), half // 2, 1)
    kept = jnp.where(second, b, a)
    out_ref[...] = jnp.where(second == low, turned, kept).astype(jnp.bfloat16)


def hidden_of(rows, gain, weights, group, most):
    n, width = rows.shape
    shards, cols, _ = weights.shape
    return pl.pallas_call(
        lambda *refs: hidden_kernel(group, most, *refs),
        grid=(shards // 2,),
        in_specs=[
            pl.BlockSpec((n, width), lambda i: (0, 0)),
            pl.BlockSpec((1, width), lambda i: (0, 0)),
            pl.BlockSpec((2, cols, width), lambda i: (i, 0, 0)),
        ],
        out_specs=pl.BlockSpec((n, cols // 2), lambda i: (0, i)),
        out_shape=jax.ShapeDtypeStruct((n, shards // 2 * cols // 2), jnp.bfloat16),
        scratch_shapes=[pltpu.VMEM((n, width), jnp.bfloat16)],
        compiler_params=pltpu.CompilerParams(dimension_semantics=("arbitrary",)),
        name="expert_hidden",
    )(rows, gain, weights)


def down_kernel(group, most, chunk, *refs):
    pieces, (down_ref, turn_ref, out_ref, y_ref) = refs[:-4], refs[-4:]
    n = pieces[0].shape[0]
    cols = out_ref.shape[1]
    second = lax.broadcasted_iota(jnp.int32, (n, cols), 0) % group >= most
    for d, piece in enumerate(pieces):
        hid = piece[...]
        first_y = jnp.dot(hid, down_ref[0], preferred_element_type=jnp.float32)
        second_y = jnp.dot(hid, down_ref[1], preferred_element_type=jnp.float32)
        y_ref[d] = jnp.where(second, second_y, first_y).astype(jnp.bfloat16)
    turn = turn_ref[...]
    size = chunk * len(pieces)
    for g in range(n // chunk):
        mixed = y_ref[:, g * chunk : (g + 1) * chunk, :].reshape(size, cols)
        out_ref[g * size : (g + 1) * size, :] = jnp.dot(
            turn, mixed, preferred_element_type=jnp.float32
        ).astype(jnp.bfloat16)


def down_of(pieces, down, group, most):
    n = pieces[0].shape[0]
    cols = down.shape[2]
    chunk = group * 8
    size = chunk * len(pieces)
    at = jnp.arange(size, dtype=jnp.int32)
    source = at % (group * len(pieces)) // group * chunk + at // (group * len(pieces)) * group
    turn = (source[:, None] + at[:, None] % group == at[None, :]).astype(jnp.bfloat16)
    return pl.pallas_call(
        lambda *refs: down_kernel(group, most, chunk, *refs),
        out_shape=jax.ShapeDtypeStruct((n * len(pieces), cols), jnp.bfloat16),
        scratch_shapes=[pltpu.VMEM((len(pieces), n, cols), jnp.bfloat16)],
        name="expert_down",
    )(*pieces, down, turn)


def body(
    out_gate,
    in_gate,
    conv_input,
    doc_ids,
    residual,
    conv_taps,
    mix_gain,
    out_weight,
    ffn_gain,
    routing,
    route_weight,
    expert_gate,
    expert_up,
    expert_down,
    shared_gate,
    shared_up,
    shared_down,
):
    f32, bf16 = jnp.float32, jnp.bfloat16
    tokens, chans = product_shape = in_gate.shape
    width = out_weight.shape[1]
    cols = residual.shape[1]
    n_tp = lax.axis_size("tp")
    n_sp = lax.axis_size("sp")
    tp = lax.axis_index("tp")
    rows = tokens // n_tp
    experts = n_sp * EXP_DEV
    most = max(1, 2 * rows * TOPK // experts)
    group = EXP_DEV * most

    gate_t, up_t = jnp.swapaxes(expert_gate, 1, 2), jnp.swapaxes(expert_up, 1, 2)
    own_weights = jnp.concatenate([gate_t, up_t], axis=0).reshape(-1, width)
    weights = lax.all_gather(own_weights, "tp", axis=0)

    product = (in_gate.astype(f32) * conv_input.astype(f32)).astype(bf16)
    last = tokens - CONV_K + 1
    docs_row = jnp.broadcast_to(doc_ids[last:, None].astype(bf16), (CONV_K - 1, LANES))
    tail = jnp.concatenate([product[last:], docs_row], axis=1)
    before = lax.ppermute(tail, "sp", [(i, i + 1) for i in range(n_sp - 1)])
    extended = jnp.concatenate([before[:, :chans], product], axis=0).astype(f32)
    ext_docs = jnp.concatenate([before[:, chans].astype(jnp.int32), doc_ids])
    mixed = jnp.zeros(product_shape, f32)
    for k in range(CONV_K):
        keep = (ext_docs[k : k + tokens] == doc_ids)[:, None]
        mixed = mixed + jnp.where(keep, conv_taps[k] * extended[k : k + tokens], f32(0.0))
    conv_out = out_gate.astype(f32) * mixed
    partial = jnp.dot(
        (conv_out * mix_gain).astype(bf16), out_weight, preferred_element_type=f32
    ).astype(bf16)

    squares = split_bf16(jnp.sum(conv_out * conv_out, axis=1, keepdims=True), 2)
    gains = jnp.stack(split_bf16(ffn_gain, 3)).reshape(rows, -1)
    gains = jnp.broadcast_to(gains[None], (n_tp, *gains.shape)).reshape(tokens, -1)
    pad = jnp.zeros((tokens, LANES - 2 - gains.shape[1]), f32)
    extra = jnp.concatenate([gains, *squares, pad], axis=1).astype(bf16)
    sent = jnp.concatenate([partial, residual, extra], axis=1).reshape(n_tp, rows, -1)
    got = lax.all_to_all(sent, "tp", 0, 0, tiled=True)
    total = jnp.sum(got[:, :, :width].astype(f32), axis=0)
    n_gain = gains.shape[1]
    sq = jnp.sum(got[:, :, width + cols + n_gain : width + cols + n_gain + 2].astype(f32), axis=(0, 2))
    own_res = jnp.moveaxis(got[:, :, width : width + cols], 0, 1).reshape(rows, width)
    scale = lax.rsqrt(sq / (chans * n_tp) + EPS)[:, None]
    stream = (own_res.astype(f32) + total * scale).astype(bf16)
    gain = got[:, :, width + cols : width + cols + n_gain].astype(f32).reshape(n_tp, 3, cols)
    gain = ((gain[:, 0] + gain[:, 1]) + gain[:, 2]).reshape(1, width)

    mine = lax.dynamic_slice_in_dim(routing, tp * rows, rows, 0).T
    slot = jnp.arange(experts * most, dtype=jnp.int32)[:, None]
    names = (mine[0:1] == slot // most) | (mine[1:2] == slot // most)
    order = jnp.arange(rows, dtype=jnp.int32)
    ahead = (order[:, None] < order[None, :]).astype(bf16)
    earlier = jnp.dot(names.astype(bf16), ahead, preferred_element_type=f32)
    pick = (names & (earlier == (slot % most).astype(f32))).astype(bf16)
    routed = jnp.dot(pick, stream, preferred_element_type=f32).astype(bf16)
    arrived = lax.all_to_all(routed.reshape(n_sp, group, width), "sp", 0, 0, tiled=True)

    everyone = lax.all_gather(stream, "tp", axis=0, tiled=True)
    every32 = everyone.astype(f32)
    mean = jnp.sum(every32 * every32, axis=1, keepdims=True) / width
    normal = (every32 * lax.rsqrt(mean + EPS) * gain).astype(bf16)
    last_dims = (((1,), (1,)), ((), ()))
    gate = lax.dot_general(shared_gate.T, normal, last_dims, preferred_element_type=f32)
    upper = lax.dot_general(shared_up.T, normal, last_dims, preferred_element_type=f32)
    shared_hid = (jax.nn.silu(gate) * upper).astype(bf16)

    hidden = hidden_of(arrived.reshape(n_sp * group, width), gain, weights, group, most)
    pieces = ring_all(hidden, "tp")
    result = down_of(pieces, expert_down, group, most)
    returned = lax.all_to_all(result, "sp", 0, 0, tiled=True)

    wide = jnp.pad(shared_hid, ((0, 0), (0, 1024 - tokens))) if tokens < 1024 else shared_hid
    hid_all = lax.all_gather(wide, "tp", axis=0, tiled=True)[:, :tokens]
    shared_part = lax.dot_general(
        hid_all, shared_down, (((0,), (0,)), ((), ())), preferred_element_type=f32
    )

    token = jnp.arange(tokens, dtype=jnp.int32)
    all_names = (routing[:, :, None] == jnp.arange(experts, dtype=jnp.int32)).astype(bf16)
    before_it = (token[:, None] > token[None, :]) & (token[:, None] // rows == token[None, :] // rows)
    counts = jnp.dot(before_it.astype(bf16), all_names.sum(axis=1), preferred_element_type=f32)
    place = jnp.sum(counts[:, None, :] * all_names.astype(f32), axis=2).astype(jnp.int32)
    block = (token // rows - tp + n_tp) % n_tp
    entry = (
        routing // EXP_DEV * (n_tp * group)
        + block[:, None] * group
        + routing % EXP_DEV * most
        + place
    )
    at = jnp.arange(n_sp * n_tp * group, dtype=jnp.int32)[None, :]
    hits = [entry[:, k : k + 1] == at for k in range(TOPK)]
    combined = shared_part
    for weight in split_bf16(route_weight, 2):
        picks = sum(jnp.where(hits[k], weight[:, k : k + 1], f32(0.0)) for k in range(TOPK))
        combined = combined + jnp.dot(
            picks.astype(bf16), returned, preferred_element_type=f32
        )
    own = lax.dynamic_slice_in_dim(everyone, tp * cols, cols, 1)
    return (own.astype(f32) + combined).astype(bf16)


def solution(mesh):
    return jax.shard_map(
        body,
        mesh=mesh,
        in_specs=(
            P(("grp", "sp"), "tp"),
            P(("grp", "sp"), "tp"),
            P(("grp", "sp"), "tp"),
            P(("grp", "sp")),
            P(("grp", "sp"), "tp"),
            P(None, "tp"),
            P("tp"),
            P("tp", None),
            P("tp"),
            P(("grp", "sp"), None),
            P(("grp", "sp"), None),
            P("sp", None, "tp"),
            P("sp", None, "tp"),
            P("sp", None, "tp"),
            P(None, "tp"),
            P(None, "tp"),
            P(None, "tp"),
        ),
        out_specs=P(("grp", "sp"), "tp"),
        check_vma=False,
    )
```

time: 413 us -> 319 us (0.77)
  waiting for transfers between devices: 287 us -> 211 us
  local copies, waits for them, and re-layouts: 23.7 us -> 7.11 us
  Pallas kernels: 0 us -> 11.4 us
  blocking collectives: 9.06 us -> 0 us
  matrix products: 14.9 us -> 8.07 us
    all_gather x3, waiting for transfers between devices: 119 us -> 39.3 us  [the longest x1 39.3 us: body(): hid_all = lax.all_gather(wide, 'tp', axis=0, tiled=True)[:, :tokens]]
    ppermute x2 -> x9, starting transfers between devices: 9 us -> 31.4 us  [the longest x3 9.83 us: ring_all(): up = lax.ppermute(up, axis, ahead)]
    all_to_all x5 -> x3, starting transfers between devices: 44.6 us -> 23.4 us  [the longest x1 9.89 us: body(): lax.all_to_all(routed.reshape(n_sp, group, width), 'sp', 0, 0, tiled=True)]
    ppermute x2 -> x9, waiting for transfers between devices: 34.9 us -> 52.6 us  [the longest x1 36.2 us: body(): before = lax.ppermute(tail, 'sp', [(i, i + 1) for i in range(n_sp - 1)])]
    all_to_all x5 -> x3, waiting for transfers between devices: 133 us -> 118 us  [the longest x1 66.1 us: body(): got = lax.all_to_all(sent, 'tp', 0, 0, tiled=True)]
    pallas_call x0 -> x2, Pallas kernels: none -> 11.4 us  [the longest x1 7.39 us: hidden_of(): pl.pallas_call(lambda *refs: hidden_kernel(group, most, *refs), grid=(sha...]
    all_to_all x1 -> x0, blocking collectives: 9.06 us -> none  [sent_to_all(): return lax.all_to_all(copies, axis, split_axis=0, concat_axis=0, tiled=True)]
    dot_general x7 -> x8, matrix products: 14.9 us -> 8.07 us  [the longest x2 2.48 us: body(): jnp.dot(picks.astype(bf16), returned, preferred_element_type=f32)]
  transfers between devices with their start and end apart: 10 -> 15, of which waited for: 8 -> 8; matrix products, arithmetic and copies ran while one was open for 4% -> 6% of each run, Pallas kernels for 0% -> 4%
where the time goes in v1:
time: 319 us; the launch traced here: 315 us
  waiting for transfers between devices  211 us (66%)
  starting transfers between devices  55.2 us (17%)
  between operations  13.7 us (4%)
  Pallas kernels  11.4 us (4%)
  other arithmetic  8.51 us (3%)
  matrix products  8.07 us (3%)
  local copies, waits for them, and re-layouts  7.11 us (2%)
    all_to_all x1, waiting for transfers between devices, body(): got = lax.all_to_all(sent, 'tp', 0, 0, tiled=True)  66.1 us
    all_to_all x1, waiting for transfers between devices, body(): lax.all_to_all(routed.reshape(n_sp, group, width), 'sp', 0, 0, tiled=True)  52.3 us
    all_gather x1, waiting for transfers between devices, body(): hid_all = lax.all_gather(wide, 'tp', axis=0, tiled=True)[:, :tokens]  39.3 us
    ppermute x1, waiting for transfers between devices, body(): before = lax.ppermute(tail, 'sp', [(i, i + 1) for i in range(n_sp - 1)])  36.2 us
    ppermute x3, waiting for transfers between devices, ring_all(): up = lax.ppermute(up, axis, ahead)  12.6 us
    all_to_all x1, starting transfers between devices, body(): lax.all_to_all(routed.reshape(n_sp, group, width), 'sp', 0, 0, tiled=True)  9.89 us
    ppermute x3, starting transfers between devices, ring_all(): up = lax.ppermute(up, axis, ahead)  9.83 us
    all_to_all x1, starting transfers between devices, body(): returned = lax.all_to_all(result, 'sp', 0, 0, tiled=True)  9.63 us
  transfers between devices with their start and end apart: 15, of which 8 were waited for; matrix products, arithmetic and copies ran while one was open for 6% of the time, Pallas kernels for 4%

profile of v1, /device:TPU:65, one launch (start us, length us, event | category | flops | bytes accessed | tf_op | source)
XLA Modules:
  0.0 315.2 jit_solution(7072092150292858609)
XLA Ops:
  6.7 2.4 pad_maximum_fusion
  9.4 7.0 %collective-permute-start = (bf16[2,256]{1,0:T(2,128)(2,1)S(1)}, bf16[2,256]{1,0:T(2,128)(2,1)S(1)}, u32[]{:S(2)}, u32[]{:S(2)}) collective-permute-start(bf16[2,256]{1,0:T(2,128)(2,1)S(1)} %pad_maximum_fusion.2), channel_id=1, source_target_pairs={{0,8},{8,16},{16,24},{24,32},{32,40},{40,48},{48,56},{56,64},{64,7... | collective-permute-start | bytes 3080 | tf_op jit(solution)/shard_map/ppermute | solution.py:166
  16.6 36.2 %collective-permute-done = bf16[2,256]{1,0:T(2,128)(2,1)S(1)} collective-permute-done((bf16[2,256]{1,0:T(2,128)(2,1)S(1)}, bf16[2,256]{1,0:T(2,128)(2,1)S(1)}, u32[]{:S(2)}, u32[]{:S(2)}) %collective-permute-start) | collective-permute-done | bytes 1056 | tf_op jit(solution)/shard_map/ppermute | solution.py:166
  53.1 0.3 multiply_reduce_fusion.1
  53.4 0.2 copy.34
  53.5 0.2 copy.35
  53.7 0.6 convolution_convert_fusion
  54.4 2.1 concatenate.24
  56.5 3.9 %all-to-all-start = ((bf16[8,48,2432]{2,1,0:T(8,128)(2,1)}), bf16[8,48,2432]{2,1,0:T(8,128)(2,1)S(1)}, u32[]{:S(2)}, u32[]{:S(2)}) async-start(bf16[8,48,2432]{2,1,0:T(8,128)(2,1)} %bitcast.44), calls=%async_computation | async-start | bytes 3735552 | tf_op jit(solution)/shard_map/all_to_all | solution.py:184
  60.5 66.1 %all-to-all-done = bf16[8,48,2432]{2,1,0:T(8,128)(2,1)S(1)} async-done(((bf16[8,48,2432]{2,1,0:T(8,128)(2,1)}), bf16[8,48,2432]{2,1,0:T(8,128)(2,1)S(1)}, u32[]{:S(2)}, u32[]{:S(2)}) %all-to-all-start) | async-done | bytes 1867808 | tf_op jit(solution)/shard_map/all_to_all | solution.py:184
  126.7 0.2 convert_reduce_fusion.1
  126.9 0.2 convert_reduce_fusion
  127.2 0.6 convolution_convert_fusion.1
  127.8 1.2 reshape.241
  129.1 9.9 %all-to-all-start.1 = ((bf16[32,6,2048]{2,1,0:T(8,128)(2,1)}), bf16[32,6,2048]{2,1,0:T(8,128)(2,1)S(1)}, u32[]{:S(2)}, u32[]{:S(2)}) async-start(bf16[32,6,2048]{2,1,0:T(8,128)(2,1)} %reshape.241), calls=%async_computation.1 | async-start | bytes 2097152 | tf_op jit(solution)/shard_map/all_to_all | solution.py:202
  139.0 0.7 all-gather.4.cloned.1.call-update
  139.8 0.7 slice_convert_fusion
  140.5 1.1 reshape.247
  141.5 0.6 slice_add_fusion
  142.2 52.3 %all-to-all-done.1 = bf16[32,6,2048]{2,1,0:T(8,128)(2,1)S(1)} async-done(((bf16[32,6,2048]{2,1,0:T(8,128)(2,1)}), bf16[32,6,2048]{2,1,0:T(8,128)(2,1)S(1)}, u32[]{:S(2)}, u32[]{:S(2)}) %all-to-all-start.1) | async-done | bytes 786464 | tf_op jit(solution)/shard_map/all_to_all | solution.py:202
  194.4 1.1 reshape.242.refs_0_
  195.6 7.4 %expert_hidden.1.refs_0_ = bf16[192,512]{1,0:T(8,128)(2,1)} custom-call(bf16[192,2048]{1,0:T(8,128)(2,1)} %reshape.242.refs_0_, f32[1,2048]{1,0:T(1,128)} %bitcast.53, bf16[8,256,2048]{2,1,0:T(8,128)(2,1)} %all-gather.8.cloned.1.call-done.refs_2_), custom_call_target="tpu_custom_call" | custom-call | tf_op jit(solution)/shard_map/expert_hidden/pallas_call | solution.py:76
  203.0 2.3 collective-permute-start.1
  205.3 3.0 collective-permute-start.5
  208.3 6.2 %collective-permute-done.1.refs_1_ = bf16[192,512]{1,0:T(8,128)(2,1)S(1)} collective-permute-done((bf16[192,512]{1,0:T(8,128)(2,1)}, bf16[192,512]{1,0:T(8,128)(2,1)S(1)}, u32[]{:S(2)}, u32[]{:S(2)}) %collective-permute-start.1) | collective-permute-done | bytes 196640 | tf_op jit(solution)/shard_map/ppermute | solution.py:31
  214.6 3.5 %collective-permute-start.2 = (bf16[192,512]{1,0:T(8,128)(2,1)S(1)}, bf16[192,512]{1,0:T(8,128)(2,1)S(1)}, u32[]{:S(2)}, u32[]{:S(2)}) collective-permute-start(bf16[192,512]{1,0:T(8,128)(2,1)S(1)} %collective-permute-done.1.refs_1_), channel_id=1, source_target_pairs={{0,7},{1,0},{2,1},{3,2},{4,3},{5,4},{6,5},{7,6},{8,15},{9,8},{10,9... | collective-permute-start | bytes 589832 | tf_op jit(solution)/shard_map/ppermute | solution.py:31
  218.1 2.4 collective-permute-start.6
  220.5 5.6 %collective-permute-done.2.refs_2_ = bf16[192,512]{1,0:T(8,128)(2,1)S(1)} collective-permute-done((bf16[192,512]{1,0:T(8,128)(2,1)S(1)}, bf16[192,512]{1,0:T(8,128)(2,1)S(1)}, u32[]{:S(2)}, u32[]{:S(2)}) %collective-permute-start.2) | collective-permute-done | bytes 196640 | tf_op jit(solution)/shard_map/ppermute | solution.py:31
  226.0 4.1 %collective-permute-start.3 = (bf16[192,512]{1,0:T(8,128)(2,1)S(1)}, bf16[192,512]{1,0:T(8,128)(2,1)S(1)}, u32[]{:S(2)}, u32[]{:S(2)}) collective-permute-start(bf16[192,512]{1,0:T(8,128)(2,1)S(1)} %collective-permute-done.2.refs_2_), channel_id=1, source_target_pairs={{0,7},{1,0},{2,1},{3,2},{4,3},{5,4},{6,5},{7,6},{8,15},{9,8},{10,9... | collective-permute-start | bytes 589832 | tf_op jit(solution)/shard_map/ppermute | solution.py:31
  230.1 2.0 collective-permute-start.7
  232.1 0.8 collective-permute-done.3.refs_3_
  232.9 5.2 %collective-permute-start.4 = (bf16[96,512]{1,0:T(8,128)(2,1)S(1)}, bf16[96,512]{1,0:T(8,128)(2,1)S(1)}, u32[]{:S(2)}, u32[]{:S(2)}) collective-permute-start(bf16[96,512]{1,0:T(8,128)(2,1)S(1)} %slice.139), channel_id=1, source_target_pairs={{0,7},{1,0},{2,1},{3,2},{4,3},{5,4},{6,5},{7,6},{8,15},{9,8},{10,9... | collective-permute-start | bytes 294920 | tf_op jit(solution)/shard_map/ppermute | solution.py:37
  238.1 2.0 collective-permute-start.8
  240.1 0.8 fusion.19.refs_9_
  240.9 3.8 %collective-permute-done.8 = bf16[96,512]{1,0:T(8,128)(2,1)S(1)} collective-permute-done((bf16[96,512]{1,0:T(8,128)(2,1)S(1)}, bf16[96,512]{1,0:T(8,128)(2,1)S(1)}, u32[]{:S(2)}, u32[]{:S(2)}) %collective-permute-start.8) | collective-permute-done | bytes 98336 | tf_op jit(solution)/shard_map/ppermute | solution.py:38
  244.7 0.7 pad_maximum_fusion.1.refs_4_
  245.5 4.0 %expert_down.1 = bf16[1536,256]{1,0:T(8,128)(2,1)} custom-call(bf16[192,512]{1,0:T(8,128)(2,1)} %expert_hidden.1.refs_0_, bf16[192,512]{1,0:T(8,128)(2,1)} %copy-done.6, bf16[192,512]{1,0:T(8,128)(2,1)} %copy-done.8, bf16[192,512]{1,0:T(8,128)(2,1)} %copy-done.3, bf16[192,512]{1,0:T(8,128)(2,1)} %pad_maximum_fusion.1.refs_4_, bf16[192,512]{1,0:T(8,128)(2,1)} %copy-done.4, ...), custom_call_target="tpu_custom_call" | custom-call | tf_op jit(solution)/shard_map/expert_down/pallas_call | solution.py:119
  249.5 9.6 %all-to-all-start.2 = ((bf16[32,48,256]{2,1,0:T(8,128)(2,1)}), bf16[32,48,256]{2,1,0:T(8,128)(2,1)S(1)}, u32[]{:S(2)}, u32[]{:S(2)}) async-start(bf16[32,48,256]{2,1,0:T(8,128)(2,1)} %bitcast.46), calls=%async_computation.2 | async-start | bytes 1572864 | tf_op jit(solution)/shard_map/all_to_all | solution.py:216
  259.2 0.2 all-gather.6.cloned.1.call-start
  259.5 1.9 fusion
  261.4 2.1 convolution_bitcast_fusion.1
  263.5 0.7 fusion.16
  264.2 0.7 pad.4
  265.0 0.3 fusion.20
  265.5 39.3 %all-gather.6.cloned.1.call-done = bf16[512,1024]{1,0:T(8,128)(2,1)} async-done(((bf16[64,1024]{1,0:T(8,128)(2,1)}), bf16[512,1024]{1,0:T(8,128)(2,1)}) %all-gather.6.cloned.1.call-update) | async-done | bytes 1048592 | tf_op jit(solution)/shard_map/all_gather | solution.py:219
  304.8 1.4 fusion.24
  306.2 1.0 convolution_add_fusion.1
  307.2 1.4 fusion.14
  (93 shorter events, 1.5 us)
Async XLA Ops:
  6.5 47.2 %copy-start = (bf16[128,2048]{1,0:T(8,128)(2,1)S(1)}, bf16[128,2048]{1,0:T(8,128)(2,1)}, u32[]{:S(2)}) copy-start(bf16[128,2048]{1,0:T(8,128)(2,1)} %param.24) | copy-start | bytes 1572868
  6.6 2.6 copy-start.12
  6.6 2.6 copy-start.11
  6.6 2.7 copy-start.15
  6.6 9.9 %copy-start.17 = (f32[3,128]{1,0:T(4,128)S(1)}, f32[3,128]{1,0:T(4,128)}, u32[]{:S(2)}) copy-start(f32[3,128]{1,0:T(4,128)} %param.22) | copy-start | bytes 4612
  6.6 9.9 %copy-start.18 = (f32[256]{0:T(256)S(1)}, f32[256]{0:T(256)}, u32[]{:S(2)}) copy-start(f32[256]{0:T(256)} %param.25) | copy-start | bytes 3076
  6.6 46.5 %copy-start.10 = (bf16[384,128]{1,0:T(8,128)(2,1)S(1)}, bf16[384,128]{1,0:T(8,128)(2,1)}, u32[]{:S(2)}) copy-start(bf16[384,128]{1,0:T(8,128)(2,1)} %param.17) | copy-start | bytes 294916
  6.6 189.0 %all-gather.8.cloned.1.call-start = ((), (), s32[]{:S(2)}) async-start(), calls=%async_computation.5 | async-start | bytes 9437184 | tf_op jit(solution)/shard_map/all_gather | solution.py:160
  6.7 47.1 %copy-start.19 = (f32[128]{0:T(128)S(1)}, f32[128]{0:T(128)}, u32[]{:S(2)}) copy-start(f32[128]{0:T(128)} %param.23) | copy-start | bytes 1540
  9.2 45.2 %copy-start.5 = (bf16[384,256]{1,0:T(8,128)(2,1)S(1)}, bf16[384,256]{1,0:T(8,128)(2,1)}, u32[]{:S(2)}) copy-start(bf16[384,256]{1,0:T(8,128)(2,1)} %param.21) | copy-start | bytes 589828
  9.4 43.4 %collective-permute-start = (bf16[2,256]{1,0:T(2,128)(2,1)S(1)}, bf16[2,256]{1,0:T(2,128)(2,1)S(1)}, u32[]{:S(2)}, u32[]{:S(2)}) collective-permute-start(bf16[2,256]{1,0:T(2,128)(2,1)S(1)} %pad_maximum_fusion.2), channel_id=1, source_target_pairs={{0,8},{8,16},{16,24},{24,32},{32,40},{40,48},{48,56},{56,64},{64,7... | collective-permute-start | bytes 3080 | tf_op jit(solution)/shard_map/ppermute | solution.py:166
  56.4 3.9 %copy-start.13 = (s32[384,2]{0,1:T(2,128)S(1)}, s32[384,2]{0,1:T(2,128)}, u32[]{:S(2)}) copy-start(s32[384,2]{0,1:T(2,128)} %param.26) | copy-start | bytes 9220
  56.5 70.1 %all-to-all-start = ((bf16[8,48,2432]{2,1,0:T(8,128)(2,1)}), bf16[8,48,2432]{2,1,0:T(8,128)(2,1)S(1)}, u32[]{:S(2)}, u32[]{:S(2)}) async-start(bf16[8,48,2432]{2,1,0:T(8,128)(2,1)} %bitcast.44), calls=%async_computation | async-start | bytes 3735552 | tf_op jit(solution)/shard_map/all_to_all | solution.py:184
  127.2 1.9 copy-start.1
  129.1 65.4 %all-to-all-start.1 = ((bf16[32,6,2048]{2,1,0:T(8,128)(2,1)}), bf16[32,6,2048]{2,1,0:T(8,128)(2,1)S(1)}, u32[]{:S(2)}, u32[]{:S(2)}) async-start(bf16[32,6,2048]{2,1,0:T(8,128)(2,1)} %reshape.241), calls=%async_computation.1 | async-start | bytes 2097152 | tf_op jit(solution)/shard_map/all_to_all | solution.py:202
  139.0 120.5 %all-gather.4.cloned.1.call-start = ((), (), s32[]{:S(2)}) async-start(), calls=%async_computation.3 | async-start | bytes 1769472 | tf_op jit(solution)/shard_map/all_gather | solution.py:204
  203.0 11.6 %collective-permute-start.1 = (bf16[192,512]{1,0:T(8,128)(2,1)}, bf16[192,512]{1,0:T(8,128)(2,1)S(1)}, u32[]{:S(2)}, u32[]{:S(2)}) collective-permute-start(bf16[192,512]{1,0:T(8,128)(2,1)} %expert_hidden.1.refs_0_), channel_id=1, source_target_pairs={{0,7},{1,0},{2,1},{3,2},{4,3},{5,4},{6,5},{7,6},{8,15},{9,8},{10,9... | collective-permute-start | bytes 589832 | tf_op jit(solution)/shard_map/ppermute | solution.py:31
  205.3 12.8 %collective-permute-start.5 = (bf16[192,512]{1,0:T(8,128)(2,1)}, bf16[192,512]{1,0:T(8,128)(2,1)S(1)}, u32[]{:S(2)}, u32[]{:S(2)}) collective-permute-start(bf16[192,512]{1,0:T(8,128)(2,1)} %expert_hidden.1.refs_0_), channel_id=1, source_target_pairs={{0,1},{1,2},{2,3},{3,4},{4,5},{5,6},{6,7},{7,0},{8,9},{9,10},{10,1... | collective-permute-start | bytes 589832 | tf_op jit(solution)/shard_map/ppermute | solution.py:32
  214.6 30.9 %copy-start.6 = (bf16[192,512]{1,0:T(8,128)(2,1)}, bf16[192,512]{1,0:T(8,128)(2,1)S(1)}, u32[]{:S(2)}) copy-start(bf16[192,512]{1,0:T(8,128)(2,1)S(1)} %collective-permute-done.1.refs_1_) | copy-start | bytes 589828
  214.6 11.5 %collective-permute-start.2 = (bf16[192,512]{1,0:T(8,128)(2,1)S(1)}, bf16[192,512]{1,0:T(8,128)(2,1)S(1)}, u32[]{:S(2)}, u32[]{:S(2)}) collective-permute-start(bf16[192,512]{1,0:T(8,128)(2,1)S(1)} %collective-permute-done.1.refs_1_), channel_id=1, source_target_pairs={{0,7},{1,0},{2,1},{3,2},{4,3},{5,4},{6,5},{7,6},{8,15},{9,8},{10,9... | collective-permute-start | bytes 589832 | tf_op jit(solution)/shard_map/ppermute | solution.py:31
  218.0 27.4 %copy-start.7 = (bf16[192,512]{1,0:T(8,128)(2,1)}, bf16[192,512]{1,0:T(8,128)(2,1)S(1)}, u32[]{:S(2)}) copy-start(bf16[192,512]{1,0:T(8,128)(2,1)S(1)} %collective-permute-done.5.refs_7_) | copy-start | bytes 589828
  218.1 12.0 %collective-permute-start.6 = (bf16[192,512]{1,0:T(8,128)(2,1)S(1)}, bf16[192,512]{1,0:T(8,128)(2,1)S(1)}, u32[]{:S(2)}, u32[]{:S(2)}) collective-permute-start(bf16[192,512]{1,0:T(8,128)(2,1)S(1)} %collective-permute-done.5.refs_7_), channel_id=1, source_target_pairs={{0,1},{1,2},{2,3},{3,4},{4,5},{5,6},{6,7},{7,0},{8,9},{9,10},{10,1... | collective-permute-start | bytes 589832 | tf_op jit(solution)/shard_map/ppermute | solution.py:32
  226.0 19.4 %copy-start.8 = (bf16[192,512]{1,0:T(8,128)(2,1)}, bf16[192,512]{1,0:T(8,128)(2,1)S(1)}, u32[]{:S(2)}) copy-start(bf16[192,512]{1,0:T(8,128)(2,1)S(1)} %collective-permute-done.2.refs_2_) | copy-start | bytes 589828
  226.0 6.9 %collective-permute-start.3 = (bf16[192,512]{1,0:T(8,128)(2,1)S(1)}, bf16[192,512]{1,0:T(8,128)(2,1)S(1)}, u32[]{:S(2)}, u32[]{:S(2)}) collective-permute-start(bf16[192,512]{1,0:T(8,128)(2,1)S(1)} %collective-permute-done.2.refs_2_), channel_id=1, source_target_pairs={{0,7},{1,0},{2,1},{3,2},{4,3},{5,4},{6,5},{7,6},{8,15},{9,8},{10,9... | collective-permute-start | bytes 589832 | tf_op jit(solution)/shard_map/ppermute | solution.py:31
  230.1 15.4 %copy-start.9 = (bf16[192,512]{1,0:T(8,128)(2,1)}, bf16[192,512]{1,0:T(8,128)(2,1)S(1)}, u32[]{:S(2)}) copy-start(bf16[192,512]{1,0:T(8,128)(2,1)S(1)} %collective-permute-done.6.refs_6_) | copy-start | bytes 589828
  230.1 8.0 %collective-permute-start.7 = (bf16[192,512]{1,0:T(8,128)(2,1)S(1)}, bf16[192,512]{1,0:T(8,128)(2,1)S(1)}, u32[]{:S(2)}, u32[]{:S(2)}) collective-permute-start(bf16[192,512]{1,0:T(8,128)(2,1)S(1)} %collective-permute-done.6.refs_6_), channel_id=1, source_target_pairs={{0,1},{1,2},{2,3},{3,4},{4,5},{5,6},{6,7},{7,0},{8,9},{9,10},{10,1... | collective-permute-start | bytes 589832 | tf_op jit(solution)/shard_map/ppermute | solution.py:32
  232.9 12.6 %copy-start.3 = (bf16[192,512]{1,0:T(8,128)(2,1)}, bf16[192,512]{1,0:T(8,128)(2,1)S(1)}, u32[]{:S(2)}) copy-start(bf16[192,512]{1,0:T(8,128)(2,1)S(1)} %collective-permute-done.3.refs_3_) | copy-start | bytes 589828
  232.9 8.0 %collective-permute-start.4 = (bf16[96,512]{1,0:T(8,128)(2,1)S(1)}, bf16[96,512]{1,0:T(8,128)(2,1)S(1)}, u32[]{:S(2)}, u32[]{:S(2)}) collective-permute-start(bf16[96,512]{1,0:T(8,128)(2,1)S(1)} %slice.139), channel_id=1, source_target_pairs={{0,7},{1,0},{2,1},{3,2},{4,3},{5,4},{6,5},{7,6},{8,15},{9,8},{10,9... | collective-permute-start | bytes 294920 | tf_op jit(solution)/shard_map/ppermute | solution.py:37
  238.1 7.4 %copy-start.4 = (bf16[192,512]{1,0:T(8,128)(2,1)}, bf16[192,512]{1,0:T(8,128)(2,1)S(1)}, u32[]{:S(2)}) copy-start(bf16[192,512]{1,0:T(8,128)(2,1)S(1)} %collective-permute-done.7.refs_5_) | copy-start | bytes 589828
  238.1 6.6 %collective-permute-start.8 = (bf16[96,512]{1,0:T(8,128)(2,1)S(1)}, bf16[96,512]{1,0:T(8,128)(2,1)S(1)}, u32[]{:S(2)}, u32[]{:S(2)}) collective-permute-start(bf16[96,512]{1,0:T(8,128)(2,1)S(1)} %slice.140), channel_id=1, source_target_pairs={{0,1},{1,2},{2,3},{3,4},{4,5},{5,6},{6,7},{7,0},{8,9},{9,10},{10,1... | collective-permute-start | bytes 294920 | tf_op jit(solution)/shard_map/ppermute | solution.py:38
  249.5 11.9 %copy-start.14 = (f32[8,1,256]{2,1,0:T(1,128)S(1)}, f32[8,1,256]{2,1,0:T(1,128)}, u32[]{:S(2)}) copy-start(f32[8,1,256]{2,1,0:T(1,128)} %slice_add_fusion) | copy-start | bytes 24580
  249.5 11.9 %copy-start.20 = (bf16[2048,64]{0,1:T(8,128)(2,1)S(1)}, bf16[2048,64]{0,1:T(8,128)(2,1)}, u32[]{:S(2)}) copy-start(bf16[2048,64]{0,1:T(8,128)(2,1)} %param.31) | copy-start | bytes 786436
  249.5 56.6 %all-to-all-start.2 = ((bf16[32,48,256]{2,1,0:T(8,128)(2,1)}), bf16[32,48,256]{2,1,0:T(8,128)(2,1)S(1)}, u32[]{:S(2)}, u32[]{:S(2)}) async-start(bf16[32,48,256]{2,1,0:T(8,128)(2,1)} %bitcast.46), calls=%async_computation.2 | async-start | bytes 1572864 | tf_op jit(solution)/shard_map/all_to_all | solution.py:216
  259.2 4.3 %copy-start.21 = (bf16[2048,64]{0,1:T(8,128)(2,1)S(1)}, bf16[2048,64]{0,1:T(8,128)(2,1)}, u32[]{:S(2)}) copy-start(bf16[2048,64]{0,1:T(8,128)(2,1)} %param.32) | copy-start | bytes 786436
  259.2 45.6 %all-gather.6.cloned.1.call-start = ((), (), s32[]{:S(2)}) async-start(), calls=%async_computation.4 | async-start | bytes 1179648 | tf_op jit(solution)/shard_map/all_gather | solution.py:219
  259.5 4.0 %copy-start.2 = (bf16[384,2048]{1,0:T(8,128)(2,1)S(1)}, bf16[384,2048]{1,0:T(8,128)(2,1)}, u32[]{:S(2)}) copy-start(bf16[384,2048]{1,0:T(8,128)(2,1)} %all-gather.4.cloned.1.call-done) | copy-start | bytes 4718596
  263.5 1.9 copy-start.16
Sparse Core Ops, SparseCore 0:
  9.5 173.9 all-gather.7
  185.6 40.1 all-gather.3
  265.1 39.6 all-gather.5

commit v2 on v1

--- a/solution.py
+++ b/solution.py
@@ -90,7 +90,7 @@
 
 
 def down_kernel(group, most, chunk, *refs):
-    pieces, (down_ref, turn_ref, out_ref, y_ref) = refs[:-4], refs[-4:]
+    pieces, (down_ref, turn_ref, _, out_ref, y_ref) = refs[:-5], refs[-5:]
     n = pieces[0].shape[0]
     cols = out_ref.shape[1]
     second = lax.broadcasted_iota(jnp.int32, (n, cols), 0) % group >= most
@@ -108,7 +108,7 @@
         ).astype(jnp.bfloat16)
 
 
-def down_of(pieces, down, group, most):
+def down_of(pieces, down, group, most, after):
     n = pieces[0].shape[0]
     cols = down.shape[2]
     chunk = group * 8
@@ -116,12 +116,14 @@
     at = jnp.arange(size, dtype=jnp.int32)
     source = at % (group * len(pieces)) // group * chunk + at // (group * len(pieces)) * group
     turn = (source[:, None] + at[:, None] % group == at[None, :]).astype(jnp.bfloat16)
+    whole = pl.BlockSpec(memory_space=pltpu.VMEM)
     return pl.pallas_call(
         lambda *refs: down_kernel(group, most, chunk, *refs),
+        in_specs=[whole] * (len(pieces) + 2) + [pl.BlockSpec(memory_space=pl.ANY)],
         out_shape=jax.ShapeDtypeStruct((n * len(pieces), cols), jnp.bfloat16),
         scratch_shapes=[pltpu.VMEM((len(pieces), n, cols), jnp.bfloat16)],
         name="expert_down",
-    )(*pieces, down, turn)
+    )(*pieces, down, turn, after)
 
 
 def body(
@@ -199,9 +201,13 @@
     earlier = jnp.dot(names.astype(bf16), ahead, preferred_element_type=f32)
     pick = (names & (earlier == (slot % most).astype(f32))).astype(bf16)
     routed = jnp.dot(pick, stream, preferred_element_type=f32).astype(bf16)
-    arrived = lax.all_to_all(routed.reshape(n_sp, group, width), "sp", 0, 0, tiled=True)
+    arrived = lax.all_to_all(routed.reshape(n_sp, most, EXP_DEV, width), "sp", 0, 0, tiled=True)
+
+    hidden = hidden_of(arrived.reshape(n_sp * group, width), gain, weights, group, most)
+    pieces = ring_all(hidden, "tp")
 
     everyone = lax.all_gather(stream, "tp", axis=0, tiled=True)
+    everyone, _ = lax.optimization_barrier((everyone, pieces[n_tp // 4]))
     every32 = everyone.astype(f32)
     mean = jnp.sum(every32 * every32, axis=1, keepdims=True) / width
     normal = (every32 * lax.rsqrt(mean + EPS) * gain).astype(bf16)
@@ -210,9 +216,7 @@
     upper = lax.dot_general(shared_up.T, normal, last_dims, preferred_element_type=f32)
     shared_hid = (jax.nn.silu(gate) * upper).astype(bf16)
 
-    hidden = hidden_of(arrived.reshape(n_sp * group, width), gain, weights, group, most)
-    pieces = ring_all(hidden, "tp")
-    result = down_of(pieces, expert_down, group, most)
+    result = down_of(pieces, expert_down, group, most, shared_hid)
     returned = lax.all_to_all(result, "sp", 0, 0, tiled=True)
 
     wide = jnp.pad(shared_hid, ((0, 0), (0, 1024 - tokens))) if tokens < 1024 else shared_hid

time: 319 us -> 325 us (1.019)
  starting transfers between devices: 55.2 us -> 60.2 us
    all_gather x1, waiting for transfers between devices: 0.02 us -> 16.2 us  [body(): everyone = lax.all_gather(stream, 'tp', axis=0, tiled=True)]
    all_to_all x1, waiting for transfers between devices: 52.3 us -> 42.8 us  [body(): lax.all_to_all(routed.reshape(n_sp, most, EXP_DEV, width), 'sp', 0, 0, ti...]
    ppermute x3, waiting for transfers between devices: 12.6 us -> 3.34 us  [ring_all(): up = lax.ppermute(up, axis, ahead)]
    all_to_all x1, starting transfers between devices: 9.63 us -> 16.1 us  [body(): returned = lax.all_to_all(result, 'sp', 0, 0, tiled=True)]
  transfers between devices with their start and end apart: 15 -> 15, of which waited for: 8 -> 9; matrix products, arithmetic and copies ran while one was open for 6% -> 6% of each run, Pallas kernels for 4% -> 2%
where the time goes in v2:
time: 325 us; the launch traced here: 322 us
  waiting for transfers between devices  211 us (65%)
  starting transfers between devices  60.2 us (19%)
  between operations  13.7 us (4%)
  Pallas kernels  11.9 us (4%)
  matrix products  11 us (3%)
  other arithmetic  7.82 us (2%)
  local copies, waits for them, and re-layouts  6.36 us (2%)
    all_to_all x1, waiting for transfers between devices, body(): got = lax.all_to_all(sent, 'tp', 0, 0, tiled=True)  66.1 us
    all_to_all x1, waiting for transfers between devices, body(): lax.all_to_all(routed.reshape(n_sp, most, EXP_DEV, width), 'sp', 0, 0, ti...  42.8 us
    all_gather x1, waiting for transfers between devices, body(): hid_all = lax.all_gather(wide, 'tp', axis=0, tiled=True)[:, :tokens]  39.2 us
    ppermute x1, waiting for transfers between devices, body(): before = lax.ppermute(tail, 'sp', [(i, i + 1) for i in range(n_sp - 1)])  36.2 us
    all_gather x1, waiting for transfers between devices, body(): everyone = lax.all_gather(stream, 'tp', axis=0, tiled=True)  16.2 us
    all_to_all x1, starting transfers between devices, body(): returned = lax.all_to_all(result, 'sp', 0, 0, tiled=True)  16.1 us
    all_to_all x1, starting transfers between devices, body(): lax.all_to_all(routed.reshape(n_sp, most, EXP_DEV, width), 'sp', 0, 0, ti...  9.89 us
    ppermute x3, starting transfers between devices, ring_all(): up = lax.ppermute(up, axis, ahead)  9.55 us
  transfers between devices with their start and end apart: 15, of which 9 were waited for; matrix products, arithmetic and copies ran while one was open for 6% of the time, Pallas kernels for 2%

profile of v2, /device:TPU:65, one launch (start us, length us, event | category | flops | bytes accessed | tf_op | source)
XLA Modules:
  0.0 322.3 jit_solution(2499957549080538461)
XLA Ops:
  6.7 2.4 pad_maximum_fusion
  9.4 7.0 %collective-permute-start = (bf16[2,256]{1,0:T(2,128)(2,1)S(1)}, bf16[2,256]{1,0:T(2,128)(2,1)S(1)}, u32[]{:S(2)}, u32[]{:S(2)}) collective-permute-start(bf16[2,256]{1,0:T(2,128)(2,1)S(1)} %pad_maximum_fusion.2), channel_id=1, source_target_pairs={{0,8},{8,16},{16,24},{24,32},{32,40},{40,48},{48,56},{56,64},{64,7... | collective-permute-start | bytes 3080 | tf_op jit(solution)/shard_map/ppermute | solution.py:168
  16.6 36.2 %collective-permute-done = bf16[2,256]{1,0:T(2,128)(2,1)S(1)} collective-permute-done((bf16[2,256]{1,0:T(2,128)(2,1)S(1)}, bf16[2,256]{1,0:T(2,128)(2,1)S(1)}, u32[]{:S(2)}, u32[]{:S(2)}) %collective-permute-start) | collective-permute-done | bytes 1056 | tf_op jit(solution)/shard_map/ppermute | solution.py:168
  52.8 0.1 convert_reduce_fusion.2
  53.1 0.3 multiply_reduce_fusion.1
  53.4 0.2 copy.34
  53.5 0.2 copy.35
  53.7 0.6 convolution_convert_fusion
  54.4 2.1 concatenate.24
  56.4 3.9 %all-to-all-start = ((bf16[8,48,2432]{2,1,0:T(8,128)(2,1)}), bf16[8,48,2432]{2,1,0:T(8,128)(2,1)S(1)}, u32[]{:S(2)}, u32[]{:S(2)}) async-start(bf16[8,48,2432]{2,1,0:T(8,128)(2,1)} %bitcast.44), calls=%async_computation | async-start | bytes 3735552 | tf_op jit(solution)/shard_map/all_to_all | solution.py:186
  60.5 66.1 %all-to-all-done = bf16[8,48,2432]{2,1,0:T(8,128)(2,1)S(1)} async-done(((bf16[8,48,2432]{2,1,0:T(8,128)(2,1)}), bf16[8,48,2432]{2,1,0:T(8,128)(2,1)S(1)}, u32[]{:S(2)}, u32[]{:S(2)}) %all-to-all-start) | async-done | bytes 1867808 | tf_op jit(solution)/shard_map/all_to_all | solution.py:186
  126.7 0.2 convert_reduce_fusion.1
  126.9 0.2 convert_reduce_fusion
  127.2 0.6 convolution_convert_fusion.1
  127.8 1.4 reshape.239
  129.2 9.9 %all-to-all-start.1 = ((bf16[32,3,2,2048]{3,2,1,0:T(2,128)(2,1)}), bf16[32,3,2,2048]{3,2,1,0:T(2,128)(2,1)S(1)}, u32[]{:S(2)}, u32[]{:S(2)}) async-start(bf16[32,3,2,2048]{3,2,1,0:T(2,128)(2,1)} %reshape.239), calls=%async_computation.1 | async-start | bytes 1572864 | tf_op jit(solution)/shard_map/all_to_all | solution.py:204
  139.2 0.7 all-gather.4.cloned.1.call-update
  139.9 0.1 reshape.247
  140.1 0.6 slice_add_fusion
  140.7 42.8 %all-to-all-done.1 = bf16[32,3,2,2048]{3,2,1,0:T(2,128)(2,1)S(1)} async-done(((bf16[32,3,2,2048]{3,2,1,0:T(2,128)(2,1)}), bf16[32,3,2,2048]{3,2,1,0:T(2,128)(2,1)S(1)}, u32[]{:S(2)}, u32[]{:S(2)}) %all-to-all-start.1) | async-done | bytes 786464 | tf_op jit(solution)/shard_map/all_to_all | solution.py:204
  183.5 1.2 reshape.240.refs_0_
  184.7 7.8 %expert_hidden.1.refs_0_ = bf16[192,512]{1,0:T(8,128)(2,1)} custom-call(bf16[192,2048]{1,0:T(8,128)(2,1)} %reshape.240.refs_0_, f32[1,2048]{1,0:T(1,128)} %bitcast.53, bf16[8,256,2048]{2,1,0:T(8,128)(2,1)} %all-gather.6.cloned.1.call-done.refs_2_), custom_call_target="tpu_custom_call" | custom-call | tf_op jit(solution)/shard_map/expert_hidden/pallas_call | solution.py:76
  192.4 2.2 collective-permute-start.1
  194.7 3.1 collective-permute-start.5
  197.8 3.3 %collective-permute-done.1.refs_1_ = bf16[192,512]{1,0:T(8,128)(2,1)S(1)} collective-permute-done((bf16[192,512]{1,0:T(8,128)(2,1)}, bf16[192,512]{1,0:T(8,128)(2,1)S(1)}, u32[]{:S(2)}, u32[]{:S(2)}) %collective-permute-start.1) | collective-permute-done | bytes 196640 | tf_op jit(solution)/shard_map/ppermute | solution.py:31
  201.2 3.2 collective-permute-start.2
  204.4 0.8 fusion.19.refs_9_
  205.2 2.4 collective-permute-done.5.refs_7_
  207.6 1.9 collective-permute-start.6
  209.6 16.2 %all-gather.4.cloned.1.call-done = bf16[384,2048]{1,0:T(8,128)(2,1)} async-done(((bf16[48,2048]{1,0:T(8,128)(2,1)}), bf16[384,2048]{1,0:T(8,128)(2,1)}) %all-gather.4.cloned.1.call-update) | async-done | bytes 1572880 | tf_op jit(solution)/shard_map/all_gather | solution.py:209
  225.8 1.9 fusion
  227.7 4.1 %collective-permute-start.3 = (bf16[192,512]{1,0:T(8,128)(2,1)S(1)}, bf16[192,512]{1,0:T(8,128)(2,1)S(1)}, u32[]{:S(2)}, u32[]{:S(2)}) collective-permute-start(bf16[192,512]{1,0:T(8,128)(2,1)S(1)} %collective-permute-done.2.refs_2_), channel_id=1, source_target_pairs={{0,7},{1,0},{2,1},{3,2},{4,3},{5,4},{6,5},{7,6},{8,15},{9,8},{10,9... | collective-permute-start | bytes 589832 | tf_op jit(solution)/shard_map/ppermute | solution.py:31
  231.8 2.0 collective-permute-start.7
  233.8 2.1 convolution_bitcast_fusion.1
  235.9 4.6 %collective-permute-start.4 = (bf16[96,512]{1,0:T(8,128)(2,1)S(1)}, bf16[96,512]{1,0:T(8,128)(2,1)S(1)}, u32[]{:S(2)}, u32[]{:S(2)}) collective-permute-start(bf16[96,512]{1,0:T(8,128)(2,1)S(1)} %slice.139), channel_id=1, source_target_pairs={{0,7},{1,0},{2,1},{3,2},{4,3},{5,4},{6,5},{7,6},{8,15},{9,8},{10,9... | collective-permute-start | bytes 294920 | tf_op jit(solution)/shard_map/ppermute | solution.py:37
  240.6 2.0 collective-permute-start.8
  242.6 2.2 fusion.16.refs_10_
  244.8 2.4 collective-permute-done.8
  247.2 0.7 pad_maximum_fusion.1.refs_4_
  247.9 4.1 %expert_down.1 = bf16[1536,256]{1,0:T(8,128)(2,1)} custom-call(bf16[192,512]{1,0:T(8,128)(2,1)} %expert_hidden.1.refs_0_, bf16[192,512]{1,0:T(8,128)(2,1)} %copy-done.6, bf16[192,512]{1,0:T(8,128)(2,1)} %copy-done.8, bf16[192,512]{1,0:T(8,128)(2,1)} %copy-done.3, bf16[192,512]{1,0:T(8,128)(2,1)} %pad_maximum_fusion.1.refs_4_, bf16[192,512]{1,0:T(8,128)(2,1)} %copy-done.4, ...), custom_call_target="tpu_custom_call" | custom-call | tf_op jit(solution)/shard_map/expert_down/pallas_call | solution.py:120
  252.0 16.1 %all-to-all-start.2 = ((bf16[32,48,256]{2,1,0:T(8,128)(2,1)}), bf16[32,48,256]{2,1,0:T(8,128)(2,1)S(1)}, u32[]{:S(2)}, u32[]{:S(2)}) async-start(bf16[32,48,256]{2,1,0:T(8,128)(2,1)} %bitcast.46), calls=%async_computation.2 | async-start | bytes 1572864 | tf_op jit(solution)/shard_map/all_to_all | solution.py:220
  268.2 0.7 pad.4
  269.0 0.3 fusion.20
  269.5 39.2 %all-gather.8.cloned.1.call-done = bf16[512,1024]{1,0:T(8,128)(2,1)} async-done(((bf16[64,1024]{1,0:T(8,128)(2,1)}), bf16[512,1024]{1,0:T(8,128)(2,1)}) %all-gather.8.cloned.1.call-update) | async-done | bytes 1048592 | tf_op jit(solution)/shard_map/all_gather | solution.py:223
  308.7 2.1 fusion.24
  310.7 1.8 all-to-all-done.2
  312.5 1.7 convolution_add_fusion.1
  314.3 1.4 fusion.14
  (93 shorter events, 1.4 us)
Async XLA Ops:
  6.5 47.2 %copy-start = (bf16[128,2048]{1,0:T(8,128)(2,1)S(1)}, bf16[128,2048]{1,0:T(8,128)(2,1)}, u32[]{:S(2)}) copy-start(bf16[128,2048]{1,0:T(8,128)(2,1)} %param.24) | copy-start | bytes 1572868
  6.6 2.6 copy-start.13
  6.6 2.6 copy-start.12
  6.6 2.7 copy-start.16
  6.6 9.9 %copy-start.18 = (f32[3,128]{1,0:T(4,128)S(1)}, f32[3,128]{1,0:T(4,128)}, u32[]{:S(2)}) copy-start(f32[3,128]{1,0:T(4,128)} %param.22) | copy-start | bytes 4612
  6.6 9.9 %copy-start.19 = (f32[256]{0:T(256)S(1)}, f32[256]{0:T(256)}, u32[]{:S(2)}) copy-start(f32[256]{0:T(256)} %param.25) | copy-start | bytes 3076
  6.6 46.5 %copy-start.11 = (bf16[384,128]{1,0:T(8,128)(2,1)S(1)}, bf16[384,128]{1,0:T(8,128)(2,1)}, u32[]{:S(2)}) copy-start(bf16[384,128]{1,0:T(8,128)(2,1)} %param.17) | copy-start | bytes 294916
  6.6 178.1 %all-gather.6.cloned.1.call-start = ((), (), s32[]{:S(2)}) async-start(), calls=%async_computation.4 | async-start | bytes 9437184 | tf_op jit(solution)/shard_map/all_gather | solution.py:162
  6.7 47.1 %copy-start.20 = (f32[128]{0:T(128)S(1)}, f32[128]{0:T(128)}, u32[]{:S(2)}) copy-start(f32[128]{0:T(128)} %param.23) | copy-start | bytes 1540
  9.2 45.2 %copy-start.5 = (bf16[384,256]{1,0:T(8,128)(2,1)S(1)}, bf16[384,256]{1,0:T(8,128)(2,1)}, u32[]{:S(2)}) copy-start(bf16[384,256]{1,0:T(8,128)(2,1)} %param.21) | copy-start | bytes 589828
  9.4 43.4 %collective-permute-start = (bf16[2,256]{1,0:T(2,128)(2,1)S(1)}, bf16[2,256]{1,0:T(2,128)(2,1)S(1)}, u32[]{:S(2)}, u32[]{:S(2)}) collective-permute-start(bf16[2,256]{1,0:T(2,128)(2,1)S(1)} %pad_maximum_fusion.2), channel_id=1, source_target_pairs={{0,8},{8,16},{16,24},{24,32},{32,40},{40,48},{48,56},{56,64},{64,7... | collective-permute-start | bytes 3080 | tf_op jit(solution)/shard_map/ppermute | solution.py:168
  56.4 3.9 %copy-start.14 = (s32[384,2]{0,1:T(2,128)S(1)}, s32[384,2]{0,1:T(2,128)}, u32[]{:S(2)}) copy-start(s32[384,2]{0,1:T(2,128)} %param.26) | copy-start | bytes 9220
  56.4 70.1 %all-to-all-start = ((bf16[8,48,2432]{2,1,0:T(8,128)(2,1)}), bf16[8,48,2432]{2,1,0:T(8,128)(2,1)S(1)}, u32[]{:S(2)}, u32[]{:S(2)}) async-start(bf16[8,48,2432]{2,1,0:T(8,128)(2,1)} %bitcast.44), calls=%async_computation | async-start | bytes 3735552 | tf_op jit(solution)/shard_map/all_to_all | solution.py:186
  127.2 12.0 %copy-start.1 = (bf16[48,2048]{1,0:T(8,128)(2,1)}, bf16[48,2048]{1,0:T(8,128)(2,1)S(1)}, u32[]{:S(2)}) copy-start(bf16[48,2048]{1,0:T(8,128)(2,1)S(1)} %add_convert_fusion.6) | copy-start | bytes 589828
  129.2 54.3 %all-to-all-start.1 = ((bf16[32,3,2,2048]{3,2,1,0:T(2,128)(2,1)}), bf16[32,3,2,2048]{3,2,1,0:T(2,128)(2,1)S(1)}, u32[]{:S(2)}, u32[]{:S(2)}) async-start(bf16[32,3,2,2048]{3,2,1,0:T(2,128)(2,1)} %reshape.239), calls=%async_computation.1 | async-start | bytes 1572864 | tf_op jit(solution)/shard_map/all_to_all | solution.py:204
  139.1 86.7 %all-gather.4.cloned.1.call-start = ((), (), s32[]{:S(2)}) async-start(), calls=%async_computation.3 | async-start | bytes 1769472 | tf_op jit(solution)/shard_map/all_gather | solution.py:209
  184.7 49.1 %copy-start.15 = (f32[8,1,256]{2,1,0:T(1,128)S(1)}, f32[8,1,256]{2,1,0:T(1,128)}, u32[]{:S(2)}) copy-start(f32[8,1,256]{2,1,0:T(1,128)} %slice_add_fusion) | copy-start | bytes 24580
  192.4 8.7 %collective-permute-start.1 = (bf16[192,512]{1,0:T(8,128)(2,1)}, bf16[192,512]{1,0:T(8,128)(2,1)S(1)}, u32[]{:S(2)}, u32[]{:S(2)}) collective-permute-start(bf16[192,512]{1,0:T(8,128)(2,1)} %expert_hidden.1.refs_0_), channel_id=1, source_target_pairs={{0,7},{1,0},{2,1},{3,2},{4,3},{5,4},{6,5},{7,6},{8,15},{9,8},{10,9... | collective-permute-start | bytes 589832 | tf_op jit(solution)/shard_map/ppermute | solution.py:31
  194.7 12.9 %collective-permute-start.5 = (bf16[192,512]{1,0:T(8,128)(2,1)}, bf16[192,512]{1,0:T(8,128)(2,1)S(1)}, u32[]{:S(2)}, u32[]{:S(2)}) collective-permute-start(bf16[192,512]{1,0:T(8,128)(2,1)} %expert_hidden.1.refs_0_), channel_id=1, source_target_pairs={{0,1},{1,2},{2,3},{3,4},{4,5},{5,6},{6,7},{7,0},{8,9},{9,10},{10,1... | collective-permute-start | bytes 589832 | tf_op jit(solution)/shard_map/ppermute | solution.py:32
  201.2 34.7 %copy-start.6 = (bf16[192,512]{1,0:T(8,128)(2,1)}, bf16[192,512]{1,0:T(8,128)(2,1)S(1)}, u32[]{:S(2)}) copy-start(bf16[192,512]{1,0:T(8,128)(2,1)S(1)} %collective-permute-done.1.refs_1_) | copy-start | bytes 589828
  201.2 24.6 %collective-permute-start.2 = (bf16[192,512]{1,0:T(8,128)(2,1)S(1)}, bf16[192,512]{1,0:T(8,128)(2,1)S(1)}, u32[]{:S(2)}, u32[]{:S(2)}) collective-permute-start(bf16[192,512]{1,0:T(8,128)(2,1)S(1)} %collective-permute-done.1.refs_1_), channel_id=1, source_target_pairs={{0,7},{1,0},{2,1},{3,2},{4,3},{5,4},{6,5},{7,6},{8,15},{9,8},{10,9... | collective-permute-start | bytes 589832 | tf_op jit(solution)/shard_map/ppermute | solution.py:31
  207.6 28.3 %copy-start.7 = (bf16[192,512]{1,0:T(8,128)(2,1)}, bf16[192,512]{1,0:T(8,128)(2,1)S(1)}, u32[]{:S(2)}) copy-start(bf16[192,512]{1,0:T(8,128)(2,1)S(1)} %collective-permute-done.5.refs_7_) | copy-start | bytes 589828
  207.6 24.2 %collective-permute-start.6 = (bf16[192,512]{1,0:T(8,128)(2,1)S(1)}, bf16[192,512]{1,0:T(8,128)(2,1)S(1)}, u32[]{:S(2)}, u32[]{:S(2)}) collective-permute-start(bf16[192,512]{1,0:T(8,128)(2,1)S(1)} %collective-permute-done.5.refs_7_), channel_id=1, source_target_pairs={{0,1},{1,2},{2,3},{3,4},{4,5},{5,6},{6,7},{7,0},{8,9},{9,10},{10,1... | collective-permute-start | bytes 589832 | tf_op jit(solution)/shard_map/ppermute | solution.py:32
  225.8 16.8 %copy-start.2 = (bf16[384,2048]{1,0:T(8,128)(2,1)S(1)}, bf16[384,2048]{1,0:T(8,128)(2,1)}, u32[]{:S(2)}) copy-start(bf16[384,2048]{1,0:T(8,128)(2,1)} %all-gather.4.cloned.1.call-done) | copy-start | bytes 4718596
  225.8 10.2 %copy-start.8 = (bf16[192,512]{1,0:T(8,128)(2,1)}, bf16[192,512]{1,0:T(8,128)(2,1)S(1)}, u32[]{:S(2)}) copy-start(bf16[192,512]{1,0:T(8,128)(2,1)S(1)} %collective-permute-done.2.refs_2_) | copy-start | bytes 589828
  227.7 8.2 %collective-permute-start.3 = (bf16[192,512]{1,0:T(8,128)(2,1)S(1)}, bf16[192,512]{1,0:T(8,128)(2,1)S(1)}, u32[]{:S(2)}, u32[]{:S(2)}) collective-permute-start(bf16[192,512]{1,0:T(8,128)(2,1)S(1)} %collective-permute-done.2.refs_2_), channel_id=1, source_target_pairs={{0,7},{1,0},{2,1},{3,2},{4,3},{5,4},{6,5},{7,6},{8,15},{9,8},{10,9... | collective-permute-start | bytes 589832 | tf_op jit(solution)/shard_map/ppermute | solution.py:31
  231.8 13.0 %copy-start.9 = (bf16[192,512]{1,0:T(8,128)(2,1)}, bf16[192,512]{1,0:T(8,128)(2,1)S(1)}, u32[]{:S(2)}) copy-start(bf16[192,512]{1,0:T(8,128)(2,1)S(1)} %collective-permute-done.6.refs_6_) | copy-start | bytes 589828
  231.8 8.7 %collective-permute-start.7 = (bf16[192,512]{1,0:T(8,128)(2,1)S(1)}, bf16[192,512]{1,0:T(8,128)(2,1)S(1)}, u32[]{:S(2)}, u32[]{:S(2)}) collective-permute-start(bf16[192,512]{1,0:T(8,128)(2,1)S(1)} %collective-permute-done.6.refs_6_), channel_id=1, source_target_pairs={{0,1},{1,2},{2,3},{3,4},{4,5},{5,6},{6,7},{7,0},{8,9},{9,10},{10,1... | collective-permute-start | bytes 589832 | tf_op jit(solution)/shard_map/ppermute | solution.py:32
  235.9 12.0 %copy-start.3 = (bf16[192,512]{1,0:T(8,128)(2,1)}, bf16[192,512]{1,0:T(8,128)(2,1)S(1)}, u32[]{:S(2)}) copy-start(bf16[192,512]{1,0:T(8,128)(2,1)S(1)} %collective-permute-done.3.refs_3_) | copy-start | bytes 589828
  235.9 8.9 %collective-permute-start.4 = (bf16[96,512]{1,0:T(8,128)(2,1)S(1)}, bf16[96,512]{1,0:T(8,128)(2,1)S(1)}, u32[]{:S(2)}, u32[]{:S(2)}) collective-permute-start(bf16[96,512]{1,0:T(8,128)(2,1)S(1)} %slice.139), channel_id=1, source_target_pairs={{0,7},{1,0},{2,1},{3,2},{4,3},{5,4},{6,5},{7,6},{8,15},{9,8},{10,9... | collective-permute-start | bytes 294920 | tf_op jit(solution)/shard_map/ppermute | solution.py:37
  240.6 7.3 %copy-start.4 = (bf16[192,512]{1,0:T(8,128)(2,1)}, bf16[192,512]{1,0:T(8,128)(2,1)S(1)}, u32[]{:S(2)}) copy-start(bf16[192,512]{1,0:T(8,128)(2,1)S(1)} %collective-permute-done.7.refs_5_) | copy-start | bytes 589828
  240.6 6.6 %collective-permute-start.8 = (bf16[96,512]{1,0:T(8,128)(2,1)S(1)}, bf16[96,512]{1,0:T(8,128)(2,1)S(1)}, u32[]{:S(2)}, u32[]{:S(2)}) collective-permute-start(bf16[96,512]{1,0:T(8,128)(2,1)S(1)} %slice.140), channel_id=1, source_target_pairs={{0,1},{1,2},{2,3},{3,4},{4,5},{5,6},{6,7},{7,0},{8,9},{9,10},{10,1... | collective-permute-start | bytes 294920 | tf_op jit(solution)/shard_map/ppermute | solution.py:38
  247.9 20.3 %copy-start.10 = (bf16[64,384]{1,0:T(8,128)(2,1)S(1)}, bf16[64,384]{1,0:T(8,128)(2,1)}, u32[]{:S(2)}) copy-start(bf16[64,384]{1,0:T(8,128)(2,1)} %fusion.16.refs_10_) | copy-start | bytes 147460
  247.9 21.5 %copy-start.17 = (f32[384,2]{0,1:T(2,128)S(1)}, f32[384,2]{0,1:T(2,128)}, u32[]{:S(2)}) copy-start(f32[384,2]{0,1:T(2,128)} %param.27) | copy-start | bytes 9220
  247.9 60.8 %copy-start.21 = (bf16[512,256]{1,0:T(8,128)(2,1)S(1)}, bf16[512,256]{1,0:T(8,128)(2,1)}, u32[]{:S(2)}) copy-start(bf16[512,256]{1,0:T(8,128)(2,1)} %param.33) | copy-start | bytes 786436
  252.0 60.5 %all-to-all-start.2 = ((bf16[32,48,256]{2,1,0:T(8,128)(2,1)}), bf16[32,48,256]{2,1,0:T(8,128)(2,1)S(1)}, u32[]{:S(2)}, u32[]{:S(2)}) async-start(bf16[32,48,256]{2,1,0:T(8,128)(2,1)} %bitcast.46), calls=%async_computation.2 | async-start | bytes 1572864 | tf_op jit(solution)/shard_map/all_to_all | solution.py:220
  268.1 40.6 %all-gather.8.cloned.1.call-start = ((), (), s32[]{:S(2)}) async-start(), calls=%async_computation.5 | async-start | bytes 1179648 | tf_op jit(solution)/shard_map/all_gather | solution.py:223
Sparse Core Ops, SparseCore 0:
  9.5 173.9 all-gather.5
  185.6 40.1 all-gather.3
  271.1 37.5 all-gather.7
